TPU v7x, 32 devices: a whole 2x2x4 slice. The times are simulated.
32 devices in a mesh: sp: 16 (over z, y, x), tp: 2 (over core).
Axes of the slice: x: 2, y: 2, z: 4, core: 2. Of those that a mesh axis runs over, the one named last changes fastest.
Arguments:
- residual: bfloat16 [2048, 2048], P(('sp', 'tp')), may hold values from -24 to 24
- query_small: bfloat16 [2048, 768], P('sp', 'tp'), may hold values from -64 to 64
- query_large: bfloat16 [2048, 1280], P('sp', 'tp'), may hold values from -64 to 64
- latent: bfloat16 [2048, 256], P('sp'), may hold values from -6 to 6
- rope_key: bfloat16 [2048, 32], P('sp'), may hold values from -48 to 48
- key_up_small: bfloat16 [256, 512], P(None, 'tp'), may hold values from -0.375 to 0.375
- value_up_small: bfloat16 [256, 512], P(None, 'tp'), may hold values from -0.375 to 0.375
- key_up_large: bfloat16 [256, 1024], P(None, 'tp'), may hold values from -0.375 to 0.375
- value_up_large: bfloat16 [256, 1024], P(None, 'tp'), may hold values from -0.375 to 0.375
- out_small: bfloat16 [512, 2048], P('tp'), may hold values from -0.625 to 0.625
- out_large: bfloat16 [1024, 2048], P('tp'), may hold values from -0.625 to 0.625
- norm_gain: bfloat16 [2048], replicated, may hold values from 0.099609375 to 1.8984375
- gate_weight: bfloat16 [2048, 5632], P('sp', 'tp'), may hold values from -0.125 to 0.125
- up_weight: bfloat16 [2048, 5632], P('sp', 'tp'), may hold values from -0.125 to 0.125
- down_weight: bfloat16 [2048, 5632], P('sp', 'tp'), may hold values from -0.21875 to 0.21875
Outputs:
- layer_out: bfloat16 [2048, 2048], P(('sp', 'tp'))
All inputs are finite; a program needn't handle non-finite values.
Results may differ from a plain program's by a relative error of at most 0.017.
Values may be sent and summed in bfloat16 or wider, within the bound.
A program may use at most 128 MiB of HBM per device.

v0:
```python
import functools
import math

import jax
import jax.numpy as jnp
import numpy as np
from jax import lax
from jax.experimental import pallas as pl
from jax.experimental.pallas import tpu as pltpu
from jax.sharding import PartitionSpec as P

MESH = pl.DeviceIdType.MESH
HEAD_SMALL = 64
HEAD_LARGE = 128
ROPE = 32
LANES = 128


big_negative = -1e30
rope_base = 500000.0
norm_eps = 1e-06


def flip(index, mask):
    bit = 1
    while bit <= mask:
        if mask & bit:
            index = index + bit * (1 - 2 * lax.rem(lax.div(index, bit), 2))
        bit *= 2
    return index


def aligned(index, size):
    return pl.multiple_of(index * size, size)


def mixer(
    plan,
    residual,
    query_small,
    query_large,
    latent,
    rope_key,
    turn_rates,
    key_up_small,
    value_up_small,
    key_up_large,
    value_up_large,
    gain,
    out_small,
    out_large,
    gate,
    up,
    down,
    out,
    keys_all,
    queries,
    bias,
    attended_small,
    attended_large,
    out_small_held,
    out_large_held,
    mixed_part,
    mixed_other,
    stream,
    gate_all,
    up_all,
    down_all,
    rows_all,
    gate_sum,
    up_sum,
    hidden,
    part,
    other,
    summed,
    arrived,
    own_sum,
    copy_sem,
    out_sem,
    far_send,
    near_send,
    weight_recv,
    keys_send,
    keys_recv,
    mixed_send,
    mixed_recv,
    rows_send,
    rows_recv,
    pair_send,
    pair_recv,
    part_send,
    part_recv,
    sum_send,
    sum_recv,
):
    far, near, tp_count, depth, tiles, wide, width = plan
    own_rows, model = residual.shape
    row_count, latent_width = latent.shape
    near_bits = near.bit_length() - 1
    chunk = near * depth
    row_total = far * tp_count * own_rows
    sp_index = lax.axis_index("sp")
    tp_index = lax.axis_index("tp")
    far_index = lax.div(sp_index, near)
    near_index = lax.rem(sp_index, near)

    def place(far_to, near_to, tp_to):
        return {"sp": far_to * near + near_to, "tp": tp_to}

    def first_tile(far_to):
        return lax.div(far_to * tiles + lax.rem(tp_index, 2) * (far - 1), far)

    def tile_count(far_to):
        return first_tile(far_to + 1) - first_tile(far_to)

    def by_count(count, act):
        if tiles % far == 0:
            act(wide)
            return
        for number in (wide - 1, wide):
            if number:
                pl.when(count == number)(functools.partial(act, number))

    inputs = (gate, up, down)
    held = (gate_all, up_all, down_all)
    own_count = tile_count(far_index)

    def source(matrix, far_to, number):
        start = aligned(first_tile(far_to), LANES)
        return inputs[matrix].at[:, pl.ds(start, number * LANES)]

    def block(matrix, far_from, near_from, number):
        start = aligned(far_from * near + near_from, depth)
        return held[matrix].at[pl.ds(start, depth), pl.ds(0, number * LANES)]

    def remote(src, dst, send, recv, device):
        return pltpu.make_async_remote_copy(
            src_ref=src,
            dst_ref=dst,
            send_sem=send,
            recv_sem=recv,
            device_id=device,
            device_id_type=MESH,
        )

    def own_copy(matrix, number):
        return pltpu.make_async_copy(
            source(matrix, far_index, number),
            block(matrix, far_index, near_index, number),
            copy_sem.at[matrix],
        )

    def far_copy(matrix, step, number):
        far_to = flip(far_index, step)
        return remote(
            source(matrix, far_to, number),
            block(matrix, far_index, near_index, number),
            far_send.at[matrix, step],
            weight_recv.at[matrix, step, 0],
            place(far_to, near_index, tp_index),
        )

    def near_order(step):
        return [(step + number) % near_bits for number in range(near_bits)]

    def near_sends(step):
        order = near_order(step)
        sends = []
        for role in range(near):
            reached = max([order.index(b) for b in range(near_bits) if role >> b & 1], default=-1)
            for bit in order[reached + 1 :]:
                sends.append((role, bit))
        return sends

    def near_copy(matrix, step, role, bit, number):
        far_from = flip(far_index, step)
        near_from = flip(near_index, role)
        target = block(matrix, far_from, near_from, number)
        direct = step == 0 and role == 0
        return remote(
            source(matrix, far_index, number) if direct else target,
            target,
            near_send.at[matrix, step, near_sends(step).index((role, bit))],
            weight_recv.at[matrix, step, role | 1 << bit],
            place(far_index, flip(near_index, 1 << bit), tp_index),
        )

    def start_far(matrix, step):
        by_count(
            tile_count(flip(far_index, step)),
            lambda number: far_copy(matrix, step, number).start(),
        )

    def forward(matrix, step, role):
        def act(number):
            for sender, bit in near_sends(step):
                if sender == role:
                    near_copy(matrix, step, role, bit, number).start()

        by_count(own_count, act)

    def await_block(matrix, step, role):
        def act(number):
            if role == 0 and step == 0:
                own_copy(matrix, number).wait()
            else:
                far_from, near_from = flip(far_index, step), flip(near_index, role)
                target = block(matrix, far_from, near_from, number)
                remote(
                    target,
                    target,
                    copy_sem.at[matrix],
                    weight_recv.at[matrix, step, role],
                    place(far_index, flip(near_index, 1), tp_index),
                ).wait_recv()

        by_count(own_count, act)

    def relay_roles(step):
        return sorted({role for role, _ in near_sends(step) if role})

    done = set()

    def take(matrices, step, role):
        for matrix in matrices:
            if (matrix, step, role) not in done:
                done.add((matrix, step, role))
                await_block(matrix, step, role)
                if not (step == 0 and role == 0):
                    forward(matrix, step, role)

    def take_group(matrices, step):
        for role in range(near):
            take(matrices, step, role)

    rates = turn_rates[...]

    def turning(first, count):
        rows = first + lax.broadcasted_iota(jnp.int32, (count, 1), 0)
        angles = rows.astype(jnp.float32) * rates
        cosine, sine = jnp.cos(angles), jnp.sin(angles)
        return (
            jnp.concatenate([cosine, cosine], axis=1),
            jnp.concatenate([-sine, sine], axis=1),
        )

    def turned(vectors, table):
        half = vectors.shape[1] // 2
        vectors = vectors.astype(jnp.float32)
        swapped = jnp.concatenate([vectors[:, half:], vectors[:, :half]], axis=1)
        return vectors * table[0] + swapped * table[1]

    first_row = sp_index * row_count
    first_own = tp_index * own_rows
    held_rows = pl.ds(aligned(tp_index, own_rows), own_rows)
    key_turn = turned(rope_key[held_rows, :], turning(first_row + first_own, own_rows))
    key_turn = key_turn.astype(jnp.bfloat16)
    key_pad = jnp.zeros((own_rows, keys_all.shape[3] - latent_width - ROPE), jnp.bfloat16)
    keys_all[tp_index, sp_index] = jnp.concatenate(
        [latent[held_rows, :], key_turn, key_pad], axis=1
    )

    if tiles % far:
        spare = pl.ds((wide - 1) * LANES, LANES)

        @pl.when(own_count < wide)
        def _():
            gate_all[:, spare] = jnp.zeros((far * chunk, LANES), gate_all.dtype)
            up_all[:, spare] = jnp.zeros((far * chunk, LANES), up_all.dtype)
            down_all[:, spare] = jnp.zeros((far * chunk, LANES), down_all.dtype)

    barrier = pltpu.get_barrier_semaphore()
    peers = [place(flip(far_index, step), near_index, tp_index) for step in range(1, far)]
    peers += [place(far_index, flip(near_index, 1 << b), tp_index) for b in range(near_bits)]
    peers += [place(far_index, near_index, flip(tp_index, j)) for j in range(1, tp_count)]
    for peer in peers:
        pl.semaphore_signal(barrier, inc=1, device_id=peer, device_id_type=MESH)
    pl.semaphore_wait(barrier, len(peers))

    def key_block(step, role):
        return keys_all.at[tp_index, flip(far_index, step) * near + flip(near_index, role)]

    def key_far(step):
        return remote(
            key_block(0, 0),
            key_block(0, 0),
            keys_send.at[step, near - 1],
            keys_recv.at[step, 0],
            place(flip(far_index, step), near_index, tp_index),
        )

    def key_near(step, role, bit):
        return remote(
            key_block(step, role),
            key_block(step, role),
            keys_send.at[step, near_sends(step).index((role, bit))],
            keys_recv.at[step, role | 1 << bit],
            place(far_index, flip(near_index, 1 << bit), tp_index),
        )

    def key_forward(step, role):
        for sender, bit in near_sends(step):
            if sender == role:
                key_near(step, role, bit).start()

    def key_take(step, role):
        remote(
            key_block(step, role),
            key_block(step, role),
            copy_sem.at[0],
            keys_recv.at[step, role],
            place(far_index, flip(near_index, 1), tp_index),
        ).wait_recv()
        key_forward(step, role)

    def key_pair(step, other_tp):
        group = keys_all.at[tp_index, pl.ds(flip(far_index, step) * near, near)]
        return remote(
            group,
            group,
            mixed_send.at[step, other_tp - 1],
            mixed_recv.at[step, other_tp - 1],
            place(far_index, near_index, flip(tp_index, other_tp)),
        )

    pairs = (0, 1)
    for step in range(1, far):
        key_far(step).start()
    key_forward(0, 0)
    for step in range(1, far):
        for matrix in pairs:
            start_far(matrix, step)
    out_copies = [
        pltpu.make_async_copy(out_small, out_small_held, out_sem.at[0]),
        pltpu.make_async_copy(out_large, out_large_held, out_sem.at[1]),
    ]
    for copy in out_copies:
        copy.start()
    for matrix in range(3):
        by_count(own_count, lambda number: own_copy(matrix, number).start())

    groups = []
    query_table = turning(first_row, row_count)
    lifted = 0
    for query, key_up, value_up, attended, size in (
        (query_small, key_up_small, value_up_small, attended_small, HEAD_SMALL),
        (query_large, key_up_large, value_up_large, attended_large, HEAD_LARGE),
    ):
        span_width = size + ROPE
        heads = query.shape[1] // span_width
        scale = float(span_width) ** -0.5 * math.log2(math.e)
        pad = jnp.zeros((row_count, keys_all.shape[3] - latent_width - ROPE), jnp.bfloat16)
        for head in range(heads):
            vector = query[:, head * span_width : (head + 1) * span_width]
            content = lax.dot_general(
                vector[:, :size],
                key_up[:, head * size : (head + 1) * size],
                (((1,), (1,)), ((), ())),
                preferred_element_type=jnp.float32,
            )
            rotary = turned(vector[:, size:], query_table)
            queries[lifted * row_count : (lifted + 1) * row_count, :] = jnp.concatenate(
                [(content * scale).astype(jnp.bfloat16), (rotary * scale).astype(jnp.bfloat16), pad],
                axis=1,
            )
            if head % 2 == 0:
                groups.append((lifted, head, min(2, heads - head), size, value_up, attended))
            lifted += 1
    key_total = tp_count * far * near * own_rows
    number = lax.broadcasted_iota(jnp.int32, (1, key_total), 1)
    key_tp = lax.div(number, far * near * own_rows)
    key_rest = lax.rem(number, far * near * own_rows)
    key_pos = (
        lax.div(key_rest, own_rows) * row_count + key_tp * own_rows + lax.rem(key_rest, own_rows)
    )
    query_pos = first_row + lax.broadcasted_iota(jnp.int32, (row_count, 1), 0)
    bias[...] = jnp.where(key_pos <= query_pos, 0.0, big_negative)

    def key_group(step):
        for role in range(1, near):
            if role not in relay_roles(step):
                key_take(step, role)
        for other_tp in range(1, tp_count):
            key_pair(step, other_tp).start()

    for step in range(1, far):
        key_take(step, 0)
        for role in relay_roles(step - 1):
            key_take(step - 1, role)
        if step > 1:
            key_group(step - 2)
    for role in relay_roles(far - 1):
        key_take(far - 1, role)
    for matrix in pairs:
        forward(matrix, 0, 0)
    for step in range(max(far - 2, 0), far):
        key_group(step)
    for step in range(far):
        for other_tp in range(1, tp_count):
            key_pair(step, other_tp).wait_recv()

    relay_plan = []
    for step in range(1, far):
        relay_plan.append((step, 0))
        for role in relay_roles(step - 1):
            relay_plan.append((step - 1, role))
    for role in relay_roles(far - 1):
        relay_plan.append((far - 1, role))

    for index, (first_head, head, count, size, value_up, attended) in enumerate(groups):
        rows = pl.ds(first_head * row_count, count * row_count)
        keys = keys_all[...].reshape(key_total, keys_all.shape[3])
        scores = lax.dot_general(
            queries[rows, :], keys, (((1,), (1,)), ((), ())), preferred_element_type=jnp.float32
        )
        masked = scores.reshape(count, row_count, key_total) + bias[...][None]
        masked = masked.reshape(count * row_count, key_total)
        weights = jnp.exp2(masked - jnp.max(masked, axis=1, keepdims=True))
        totals = jnp.sum(weights, axis=1, keepdims=True)
        gathered = jnp.dot(
            weights.astype(jnp.bfloat16),
            keys[:, :latent_width],
            preferred_element_type=jnp.float32,
        )
        gathered = (gathered / totals).astype(jnp.bfloat16)
        values = [
            jnp.dot(
                gathered[place_of * row_count : (place_of + 1) * row_count],
                value_up[:, (head + place_of) * size : (head + place_of + 1) * size],
                preferred_element_type=jnp.float32,
            ).astype(jnp.bfloat16)
            for place_of in range(count)
        ]
        attended[:, head * size : (head + count) * size] = jnp.concatenate(values, axis=1)
        if relay_plan:
            take(pairs, *relay_plan.pop(0))

    for copy in out_copies:
        copy.wait()
    share = jnp.dot(
        attended_small[...], out_small_held[...], preferred_element_type=jnp.float32
    ) + jnp.dot(attended_large[...], out_large_held[...], preferred_element_type=jnp.float32)
    mixed_part[...] = share.reshape(tp_count, own_rows, model)

    def mixed_copy(other_tp):
        tp_to = flip(tp_index, other_tp)
        return remote(
            mixed_other.at[0, other_tp - 1],
            mixed_other.at[1, other_tp - 1],
            mixed_send.at[far, other_tp - 1],
            mixed_recv.at[far, other_tp - 1],
            place(far_index, near_index, tp_to),
        )

    for other_tp in range(1, tp_count):
        mixed_other[0, other_tp - 1] = mixed_part[flip(tp_index, other_tp)].astype(jnp.bfloat16)
        mixed_copy(other_tp).start()
    mixed = mixed_part[tp_index]
    for other_tp in range(1, tp_count):
        mixed_copy(other_tp).wait_recv()
        mixed = mixed + mixed_other[1, other_tp - 1].astype(jnp.float32)
    mixed = mixed.astype(jnp.bfloat16).astype(jnp.float32)
    stream[...] = (residual[...].astype(jnp.float32) + mixed).astype(jnp.bfloat16)
    as_float = stream[...].astype(jnp.float32)
    spread = lax.rsqrt(jnp.mean(as_float * as_float, axis=1, keepdims=True) + norm_eps)
    normed = as_float * spread * gain[...].astype(jnp.float32)
    rows_all[far_index, tp_index] = normed.astype(jnp.bfloat16)

    def rows_copy(step):
        return remote(
            rows_all.at[far_index, tp_index],
            rows_all.at[far_index, tp_index],
            rows_send.at[step],
            rows_recv.at[step],
            place(flip(far_index, step), near_index, tp_index),
        )

    def pair_copy(step, other_tp):
        far_from = flip(far_index, step)
        target = rows_all.at[far_from, tp_index]
        return remote(
            target,
            target,
            pair_send.at[step, other_tp - 1],
            pair_recv.at[step, other_tp - 1],
            place(far_index, near_index, flip(tp_index, other_tp)),
        )

    for step in range(1, far):
        rows_copy(step).start()
    for other_tp in range(1, tp_count):
        pair_copy(0, other_tp).start()

    for step in range(1, far):
        start_far(2, step)

    while relay_plan:
        take(pairs, *relay_plan.pop(0))
    forward(2, 0, 0)
    for step in range(1, far):
        rows_copy(step).wait_recv()
        for other_tp in range(1, tp_count):
            pair_copy(step, other_tp).start()
    for step in range(far):
        for other_tp in range(1, tp_count):
            pair_copy(step, other_tp).wait_recv()

    tile = 2 * LANES if width % (2 * LANES) == 0 else LANES
    for step in range(far):
        take_group(pairs, step)
        if step == far - 1:
            take((2,), 1, 0)
        start = aligned(flip(far_index, step), chunk)
        rows = rows_all[:, :, :, pl.ds(start, chunk)].reshape(row_total, chunk)
        for first in range(0, width, tile):
            span = pl.ds(first, tile)
            for weight, total in ((gate_all, gate_sum), (up_all, up_sum)):
                product = jnp.dot(
                    rows, weight[pl.ds(start, chunk), span], preferred_element_type=jnp.float32
                )
                total[:, span] = product if step == 0 else total[:, span] + product
    for first in range(0, width, LANES):
        span = pl.ds(first, LANES)
        value = gate_sum[:, span]
        value = (value / (1.0 + jnp.exp(-value)) * up_sum[:, span]).astype(hidden.dtype)
        if first >= (wide - 1) * LANES and tiles % far:
            value = jnp.where(own_count == wide, value, jnp.zeros_like(value))
        hidden[:, span] = value

    def part_copy(step, other_tp):
        tp_to = flip(tp_index, other_tp)
        return remote(
            part.at[step, :, tp_to],
            other.at[step, other_tp - 1],
            part_send.at[step, other_tp - 1],
            part_recv.at[step, other_tp - 1],
            place(far_index, near_index, tp_to),
        )

    def sum_copy(step, apart):
        far_to = flip(far_index, apart)
        return remote(
            summed.at[step, far_to],
            arrived.at[apart - 1, flip(far_index, step)],
            sum_send.at[step, apart - 1],
            sum_recv.at[step, apart - 1],
            place(far_to, near_index, tp_index),
        )

    def finish(step):
        total = part[step, :, tp_index].astype(jnp.float32)
        for other_tp in range(1, tp_count):
            part_copy(step, other_tp).wait_recv()
            total = total + other[step, other_tp - 1].astype(jnp.float32)
        summed[step] = total.astype(summed.dtype)
        for apart in range(1, far):
            sum_copy(step, apart).start()
        own_sum[flip(far_index, step)] = summed[step, far_index]

    for step in range(1, far):
        take((2,), step, 0)
        for role in relay_roles(step - 1):
            take((2,), step - 1, role)
    for role in relay_roles(far - 1):
        take((2,), far - 1, role)
    for step in range(far):
        take_group((2,), step)
        start = aligned(flip(far_index, step), chunk)
        product = lax.dot_general(
            hidden[...],
            down_all[pl.ds(start, chunk), :],
            (((1,), (1,)), ((), ())),
            preferred_element_type=jnp.float32,
        )
        part[step] = product.reshape(far, tp_count, own_rows, chunk).astype(part.dtype)
        for other_tp in range(1, tp_count):
            part_copy(step, other_tp).start()
        if step:
            finish(step - 1)
    finish(far - 1)

    for step in range(far):
        for apart in range(1, far):
            remote(
                summed.at[step, 0],
                arrived.at[apart - 1, flip(flip(far_index, apart), step)],
                sum_send.at[step, apart - 1],
                sum_recv.at[step, apart - 1],
                place(flip(far_index, apart), near_index, tp_index),
            ).wait_recv()
    for place_of in range(far):
        span = pl.ds(place_of * chunk, chunk)
        channel = own_sum[place_of].astype(jnp.float32)
        for apart in range(1, far):
            channel = channel + arrived[apart - 1, place_of].astype(jnp.float32)
        channel = channel.astype(jnp.bfloat16).astype(jnp.float32)
        out[:, span] = (stream[:, span].astype(jnp.float32) + 0.5 * channel).astype(out.dtype)

    for step in range(far):
        if step:
            key_far(step).wait_send()
        for role, bit in near_sends(step):
            key_near(step, role, bit).wait_send()
        for other_tp in range(1, tp_count):
            key_pair(step, other_tp).wait_send()
    for other_tp in range(1, tp_count):
        mixed_copy(other_tp).wait_send()
    for matrix in range(3):
        for step in range(1, far):
            by_count(
                tile_count(flip(far_index, step)),
                lambda number: far_copy(matrix, step, number).wait_send(),
            )
        for step in range(far):
            for role, bit in near_sends(step):
                by_count(
                    own_count,
                    lambda number: near_copy(matrix, step, role, bit, number).wait_send(),
                )
    for step in range(far):
        if step:
            rows_copy(step).wait_send()
        for other_tp in range(1, tp_count):
            pair_copy(step, other_tp).wait_send()
            part_copy(step, other_tp).wait_send()
        for apart in range(1, far):
            sum_copy(step, apart).wait_send()


def shards(
    residual,
    query_small,
    query_large,
    latent,
    rope_key,
    key_up_small,
    value_up_small,
    key_up_large,
    value_up_large,
    out_small,
    out_large,
    norm_gain,
    gate_weight,
    up_weight,
    down_weight,
):
    sp_count = lax.axis_size("sp")
    tp_count = lax.axis_size("tp")
    far = 1
    while far * far < sp_count:
        far *= 2
    near = sp_count // far
    spare = -gate_weight.shape[1] % LANES
    if spare:
        gate_weight, up_weight, down_weight = (
            jnp.pad(weight, ((0, 0), (0, spare))) for weight in (gate_weight, up_weight, down_weight)
        )
    own_rows, model = residual.shape
    row_count, latent_width = latent.shape
    depth, units = gate_weight.shape
    tiles = units // LANES
    wide = -(-tiles // far)
    width = wide * LANES
    chunk = near * depth
    row_total = far * tp_count * own_rows
    key_total = sp_count * row_count
    key_width = -(-(latent_width + ROPE) // LANES) * LANES
    small, large = out_small.shape[0], out_large.shape[0]
    heads = small // HEAD_SMALL + large // HEAD_LARGE
    rates = 1.0 / rope_base ** (np.arange(0, ROPE, 2, dtype=np.float32) / ROPE)
    plan = (far, near, tp_count, depth, tiles, wide, width)
    bf16, f32 = jnp.bfloat16, jnp.float32
    others = max(tp_count - 1, 1)
    dma = pltpu.SemaphoreType.DMA
    vmem = pl.BlockSpec(memory_space=pltpu.VMEM)
    anywhere = pl.BlockSpec(memory_space=pl.ANY)
    return pl.pallas_call(
        functools.partial(mixer, plan),
        out_shape=jax.ShapeDtypeStruct((own_rows, model), bf16),
        in_specs=[vmem] * 11 + [anywhere] * 5,
        out_specs=vmem,
        scratch_shapes=[
            pltpu.VMEM((tp_count, sp_count, own_rows, key_width), bf16),
            pltpu.VMEM((heads * row_count, key_width), bf16),
            pltpu.VMEM((row_count, key_total), f32),
            pltpu.VMEM((row_count, small), bf16),
            pltpu.VMEM((row_count, large), bf16),
            pltpu.VMEM(out_small.shape, bf16),
            pltpu.VMEM(out_large.shape, bf16),
            pltpu.VMEM((tp_count, own_rows, model), f32),
            pltpu.VMEM((2, others, own_rows, model), bf16),
            pltpu.VMEM((own_rows, model), bf16),
            pltpu.VMEM((model, width), bf16),
            pltpu.VMEM((model, width), bf16),
            pltpu.VMEM((model, width), bf16),
            pltpu.VMEM((far, tp_count, own_rows, model), bf16),
            pltpu.VMEM((row_total, width), f32),
            pltpu.VMEM((row_total, width), f32),
            pltpu.VMEM((row_total, width), bf16),
            pltpu.VMEM((far, far, tp_count, own_rows, chunk), bf16),
            pltpu.VMEM((far, others, far, own_rows, chunk), bf16),
            pltpu.VMEM((far, far, own_rows, chunk), bf16),
            pltpu.VMEM((far - 1, far, own_rows, chunk), bf16),
            pltpu.VMEM((far, own_rows, chunk), bf16),
            dma((3,)),
            dma((2,)),
            dma((3, far)),
            dma((3, far, near - 1)),
            dma((3, far, near)),
            dma((far, near)),
            dma((far, near)),
            dma((far + 1, others)),
            dma((far + 1, others)),
            dma((far,)),
            dma((far,)),
            dma((far, others)),
            dma((far, others)),
            dma((far, others)),
            dma((far, others)),
            dma((far, far - 1)),
            dma((far, far - 1)),
        ],
        compiler_params=pltpu.CompilerParams(
            collective_id=0, has_side_effects=True, vmem_limit_bytes=58 * 1024 * 1024
        ),
    )(
        residual,
        query_small,
        query_large,
        latent,
        rope_key,
        jnp.asarray(rates[None, :], f32),
        key_up_small,
        value_up_small,
        key_up_large,
        value_up_large,
        norm_gain[None, :],
        out_small,
        out_large,
        gate_weight,
        up_weight,
        down_weight,
    )


def solution(mesh):
    placed = (
        P(("sp", "tp"), None),
        P("sp", "tp"),
        P("sp", "tp"),
        P("sp", None),
        P("sp", None),
        P(None, "tp"),
        P(None, "tp"),
        P(None, "tp"),
        P(None, "tp"),
        P("tp", None),
        P("tp", None),
        P(),
        P("sp", "tp"),
        P("sp", "tp"),
        P("sp", "tp"),
    )
    return jax.shard_map(
        shards, mesh=mesh, in_specs=placed, out_specs=P(("sp", "tp"), None), check_vma=False
    )
```

profile of v0, /device:TPU:0, one launch (start us, length us, event | category | flops | bytes accessed | tf_op | source)
XLA Modules:
  0.0 124.8 jit_solution(3745329805909196266)
XLA Ops:
  0.0 1.3 %broadcast_in_dim.3.gain = bf16[1,2048]{1,0:T(2,128)(2,1)} reshape(bf16[2048]{0:T(1024)(128)(2,1)} %param.27) | data formatting | bytes 8192 | tf_op jit(solution)/shard_map/broadcast_in_dim | solution.py:737
  1.3 1.4 %copy.17.rope_key = bf16[128,32]{1,0:T(8,128)(2,1)} copy(bf16[128,32]{0,1:T(8,128)(2,1)} %param.20) | data formatting | bytes 16384 | tf_op args[4]
  2.7 120.5 %shard_map.154 = bf16[64,2048]{1,0:T(8,128)(2,1)} custom-call(bf16[64,2048]{1,0:T(8,128)(2,1)} %residual.1, bf16[128,384]{1,0:T(8,128)(2,1)} %query_small.1, bf16[128,640]{1,0:T(8,128)(2,1)} %query_large.1, bf16[128,256]{1,0:T(8,128)(2,1)} %latent.1, bf16[128,32]{1,0:T(8,128)(2,1)} %copy.17.rope_key, f32[1,16]{1,0:T(1,128)} %constant.2.clone.turn_rates, ...), custom_call_target="tpu_custom_call" | custom-call | tf_op jit(solution)/shard_map/pallas_call | solution.py:677
  123.2 1.7 %copy.19 = bf16[64,2048]{1,0:T(8,128)(2,1)} copy(bf16[64,2048]{1,0:T(8,128)(2,1)} %shard_map.154) | data formatting | bytes 524288
where the time goes:
time: 125 us
  Pallas kernels  120 us (96%)
  local copies, waits for them, and re-layouts  4.36 us (3%)
    pallas_call x1, Pallas kernels, shards(): pl.pallas_call(functools.partial(mixer, plan), out_shape=jax.ShapeDtypeSt...  120 us
    unnamed x2, local copies, waits for them, and re-layouts  3.08 us

commit v1 on v0

--- a/solution.py
+++ b/solution.py
@@ -53,6 +53,7 @@
     up,
     down,
     out,
+    keys_own,
     keys_all,
     queries,
     bias,
@@ -180,7 +181,7 @@
         return remote(
             source(matrix, far_index, number) if direct else target,
             target,
-            near_send.at[matrix, step, near_sends(step).index((role, bit))],
+            near_send.at[matrix, step, near_sends(step + matrix).index((role, bit))],
             weight_recv.at[matrix, step, role | 1 << bit],
             place(far_index, flip(near_index, 1 << bit), tp_index),
         )
@@ -193,13 +194,17 @@
 
     def forward(matrix, step, role):
         def act(number):
-            for sender, bit in near_sends(step):
+            for sender, bit in near_sends(step + matrix):
                 if sender == role:
                     near_copy(matrix, step, role, bit, number).start()
 
         by_count(own_count, act)
 
     def await_block(matrix, step, role):
+        with jax.named_scope(f"wait_m{matrix}_s{step}_r{role}"):
+            await_block_(matrix, step, role)
+
+    def await_block_(matrix, step, role):
         def act(number):
             if role == 0 and step == 0:
                 own_copy(matrix, number).wait()
@@ -229,10 +234,21 @@
                 if not (step == 0 and role == 0):
                     forward(matrix, step, role)
 
+    def relay(matrices, step):
+        for matrix in matrices:
+            for role in relay_roles(step + matrix):
+                take((matrix,), step, role)
+
     def take_group(matrices, step):
         for role in range(near):
             take(matrices, step, role)
 
+    barrier = pltpu.get_barrier_semaphore()
+    peers = [place(flip(far_index, step), near_index, tp_index) for step in range(1, far)]
+    peers += [place(far_index, flip(near_index, 1 << b), tp_index) for b in range(near_bits)]
+    peers += [place(far_index, near_index, flip(tp_index, j)) for j in range(1, tp_count)]
+    for peer in peers:
+        pl.semaphore_signal(barrier, inc=1, device_id=peer, device_id_type=MESH)
     rates = turn_rates[...]
 
     def turning(first, count):
@@ -251,14 +267,12 @@
         return vectors * table[0] + swapped * table[1]
 
     first_row = sp_index * row_count
-    first_own = tp_index * own_rows
-    held_rows = pl.ds(aligned(tp_index, own_rows), own_rows)
-    key_turn = turned(rope_key[held_rows, :], turning(first_row + first_own, own_rows))
-    key_turn = key_turn.astype(jnp.bfloat16)
-    key_pad = jnp.zeros((own_rows, keys_all.shape[3] - latent_width - ROPE), jnp.bfloat16)
-    keys_all[tp_index, sp_index] = jnp.concatenate(
-        [latent[held_rows, :], key_turn, key_pad], axis=1
-    )
+    query_table = turning(first_row, row_count)
+    key_turn = turned(rope_key[...].T, query_table).astype(jnp.bfloat16)
+    key_pad = jnp.zeros((row_count, keys_all.shape[3] - latent_width - ROPE), jnp.bfloat16)
+    own_keys = jnp.concatenate([latent[...], key_turn, key_pad], axis=1)
+    keys_own[...] = own_keys.reshape(tp_count, own_rows, keys_all.shape[3])
+    keys_all[tp_index, sp_index] = keys_own[tp_index]
 
     if tiles % far:
         spare = pl.ds((wide - 1) * LANES, LANES)
@@ -269,13 +283,8 @@
             up_all[:, spare] = jnp.zeros((far * chunk, LANES), up_all.dtype)
             down_all[:, spare] = jnp.zeros((far * chunk, LANES), down_all.dtype)
 
-    barrier = pltpu.get_barrier_semaphore()
-    peers = [place(flip(far_index, step), near_index, tp_index) for step in range(1, far)]
-    peers += [place(far_index, flip(near_index, 1 << b), tp_index) for b in range(near_bits)]
-    peers += [place(far_index, near_index, flip(tp_index, j)) for j in range(1, tp_count)]
-    for peer in peers:
-        pl.semaphore_signal(barrier, inc=1, device_id=peer, device_id_type=MESH)
-    pl.semaphore_wait(barrier, len(peers))
+    with jax.named_scope('barrier'):
+        pl.semaphore_wait(barrier, len(peers))
 
     def key_block(step, role):
         return keys_all.at[tp_index, flip(far_index, step) * near + flip(near_index, role)]
@@ -304,6 +313,7 @@
                 key_near(step, role, bit).start()
 
     def key_take(step, role):
+      with jax.named_scope(f"wait_key_s{step}_r{role}"):
         remote(
             key_block(step, role),
             key_block(step, role),
@@ -327,9 +337,20 @@
     for step in range(1, far):
         key_far(step).start()
     key_forward(0, 0)
-    for step in range(1, far):
-        for matrix in pairs:
-            start_far(matrix, step)
+    for matrix in pairs:
+        forward(matrix, 0, 0)
+    for matrix in pairs:
+        start_far(matrix, 1)
+    inner = lax.rem(lax.div(far_index, max(far // 2, 1)) + lax.div(far_index, max(far // 4, 1)), 2)
+
+    def start_rest(steps):
+        for step in steps:
+            for matrix in pairs:
+                start_far(matrix, step)
+
+    pl.when(inner == 0)(lambda: start_rest(range(2, far)))
+    pl.when(inner == 1)(lambda: start_rest(range(far - 1, 1, -1)))
+    start_far(2, 1)
     out_copies = [
         pltpu.make_async_copy(out_small, out_small_held, out_sem.at[0]),
         pltpu.make_async_copy(out_large, out_large_held, out_sem.at[1]),
@@ -340,7 +361,6 @@
         by_count(own_count, lambda number: own_copy(matrix, number).start())
 
     groups = []
-    query_table = turning(first_row, row_count)
     lifted = 0
     for query, key_up, value_up, attended, size in (
         (query_small, key_up_small, value_up_small, attended_small, HEAD_SMALL),
@@ -389,23 +409,17 @@
             key_take(step - 1, role)
         if step > 1:
             key_group(step - 2)
+    relay(pairs, 0)
     for role in relay_roles(far - 1):
         key_take(far - 1, role)
-    for matrix in pairs:
-        forward(matrix, 0, 0)
+    take(pairs, 1, 0)
+    forward(2, 0, 0)
     for step in range(max(far - 2, 0), far):
         key_group(step)
     for step in range(far):
         for other_tp in range(1, tp_count):
-            key_pair(step, other_tp).wait_recv()
-
-    relay_plan = []
-    for step in range(1, far):
-        relay_plan.append((step, 0))
-        for role in relay_roles(step - 1):
-            relay_plan.append((step - 1, role))
-    for role in relay_roles(far - 1):
-        relay_plan.append((far - 1, role))
+            with jax.named_scope('wait_keypair'):
+                key_pair(step, other_tp).wait_recv()
 
     for index, (first_head, head, count, size, value_up, attended) in enumerate(groups):
         rows = pl.ds(first_head * row_count, count * row_count)
@@ -431,12 +445,14 @@
             ).astype(jnp.bfloat16)
             for place_of in range(count)
         ]
-        attended[:, head * size : (head + count) * size] = jnp.concatenate(values, axis=1)
-        if relay_plan:
-            take(pairs, *relay_plan.pop(0))
+        with jax.named_scope(f"att_done{index}"):
+            attended[:, head * size : (head + count) * size] = jnp.concatenate(values, axis=1)
+        if index == len(groups) - 1:
+            relay(pairs, 1)
 
     for copy in out_copies:
-        copy.wait()
+        with jax.named_scope('outcopy'):
+            copy.wait()
     share = jnp.dot(
         attended_small[...], out_small_held[...], preferred_element_type=jnp.float32
     ) + jnp.dot(attended_large[...], out_large_held[...], preferred_element_type=jnp.float32)
@@ -455,61 +471,102 @@
     for other_tp in range(1, tp_count):
         mixed_other[0, other_tp - 1] = mixed_part[flip(tp_index, other_tp)].astype(jnp.bfloat16)
         mixed_copy(other_tp).start()
+    for step in range(2, far):
+        take(pairs, step, 0)
     mixed = mixed_part[tp_index]
     for other_tp in range(1, tp_count):
-        mixed_copy(other_tp).wait_recv()
+        with jax.named_scope('wait_mixed'):
+            mixed_copy(other_tp).wait_recv()
         mixed = mixed + mixed_other[1, other_tp - 1].astype(jnp.float32)
     mixed = mixed.astype(jnp.bfloat16).astype(jnp.float32)
     stream[...] = (residual[...].astype(jnp.float32) + mixed).astype(jnp.bfloat16)
     as_float = stream[...].astype(jnp.float32)
     spread = lax.rsqrt(jnp.mean(as_float * as_float, axis=1, keepdims=True) + norm_eps)
-    normed = as_float * spread * gain[...].astype(jnp.float32)
-    rows_all[far_index, tp_index] = normed.astype(jnp.bfloat16)
-
-    def rows_copy(step):
-        return remote(
-            rows_all.at[far_index, tp_index],
-            rows_all.at[far_index, tp_index],
-            rows_send.at[step],
-            rows_recv.at[step],
-            place(flip(far_index, step), near_index, tp_index),
-        )
-
-    def pair_copy(step, other_tp):
-        far_from = flip(far_index, step)
-        target = rows_all.at[far_from, tp_index]
-        return remote(
-            target,
-            target,
-            pair_send.at[step, other_tp - 1],
-            pair_recv.at[step, other_tp - 1],
+    normed = as_float * spread * gain[...].astype(jnp.float32).reshape(1, model)
+    with jax.named_scope('normed'):
+        rows_all[far_index, tp_index] = normed.astype(jnp.bfloat16)
+
+    far_bits = far.bit_length() - 1
+    pieces = 2 if model % (2 * LANES) == 0 else 1
+    piece_width = model // pieces
+
+    def rows_sends():
+        sends = []
+        for role in range(far):
+            low = min([b for b in range(far_bits) if role >> b & 1], default=far_bits)
+            sends += [(role, bit) for bit in reversed(range(low))]
+        return sends
+
+    def rows_part(role, piece):
+        span = pl.ds(piece * piece_width, piece_width)
+        return rows_all.at[flip(far_index, role), tp_index, :, span]
+
+    def rows_copy(role, bit, piece):
+        return remote(
+            rows_part(role, piece),
+            rows_part(role, piece),
+            rows_send.at[rows_sends().index((role, bit)), piece],
+            rows_recv.at[role | 1 << bit, piece],
+            place(flip(far_index, 1 << bit), near_index, tp_index),
+        )
+
+    def pair_copy(role, other_tp, piece):
+        return remote(
+            rows_part(role, piece),
+            rows_part(role, piece),
+            pair_send.at[role, other_tp - 1, piece],
+            pair_recv.at[role, other_tp - 1, piece],
             place(far_index, near_index, flip(tp_index, other_tp)),
         )
 
-    for step in range(1, far):
-        rows_copy(step).start()
-    for other_tp in range(1, tp_count):
-        pair_copy(0, other_tp).start()
-
-    for step in range(1, far):
+    def rows_pass(role, piece):
+        for sender, bit in rows_sends():
+            if sender == role:
+                rows_copy(role, bit, piece).start()
+        for other_tp in range(1, tp_count):
+            pair_copy(role, other_tp, piece).start()
+
+    def rows_take(role):
+        for piece in range(pieces):
+            with jax.named_scope(f"wait_rows{role}_{piece}"):
+                remote(
+                    rows_part(role, piece),
+                    rows_part(role, piece),
+                    copy_sem.at[0],
+                    rows_recv.at[role, piece],
+                    place(flip(far_index, 1), near_index, tp_index),
+                ).wait_recv()
+            rows_pass(role, piece)
+
+    for piece in range(pieces):
+        rows_pass(0, piece)
+    for step in reversed(range(3, far)):
         start_far(2, step)
-
-    while relay_plan:
-        take(pairs, *relay_plan.pop(0))
-    forward(2, 0, 0)
-    for step in range(1, far):
-        rows_copy(step).wait_recv()
+    relayed = sorted({role for role, _ in rows_sends() if role}, reverse=True)
+    leaves = [role for role in range(1, far) if role not in relayed]
+    relay((2,), 0)
+    for step in range(2, far // 2 + 1):
+        relay(pairs, step)
+    for role in relayed:
+        rows_take(role)
+    if far > 2:
+        start_far(2, 2)
+    for step in range(far // 2 + 1, far):
+        relay(pairs, step)
+    take((2,), 1, 0)
+    for role in leaves:
+        rows_take(role)
+    for step in reversed(range(3, far)):
+        take((2,), step, 0)
+    for role in range(far):
         for other_tp in range(1, tp_count):
-            pair_copy(step, other_tp).start()
-    for step in range(far):
-        for other_tp in range(1, tp_count):
-            pair_copy(step, other_tp).wait_recv()
+            for piece in range(pieces):
+                with jax.named_scope(f"wait_pair{role}"):
+                    pair_copy(role, other_tp, piece).wait_recv()
 
     tile = 2 * LANES if width % (2 * LANES) == 0 else LANES
     for step in range(far):
         take_group(pairs, step)
-        if step == far - 1:
-            take((2,), 1, 0)
         start = aligned(flip(far_index, step), chunk)
         rows = rows_all[:, :, :, pl.ds(start, chunk)].reshape(row_total, chunk)
         for first in range(0, width, tile):
@@ -527,69 +584,85 @@
             value = jnp.where(own_count == wide, value, jnp.zeros_like(value))
         hidden[:, span] = value
 
-    def part_copy(step, other_tp):
+    half = chunk // 2
+
+    def columns_of(step, side):
+        top = near // 2
+        return flip(far_index, step) * 2 + lax.rem(lax.div(near_index, top) + side, 2)
+
+    def part_copy(step, side, other_tp):
         tp_to = flip(tp_index, other_tp)
         return remote(
-            part.at[step, :, tp_to],
-            other.at[step, other_tp - 1],
-            part_send.at[step, other_tp - 1],
-            part_recv.at[step, other_tp - 1],
+            part.at[step * 2 + side, :, tp_to],
+            other.at[step * 2 + side, other_tp - 1],
+            part_send.at[step * 2 + side, other_tp - 1],
+            part_recv.at[step * 2 + side, other_tp - 1],
             place(far_index, near_index, tp_to),
         )
 
-    def sum_copy(step, apart):
+    def sum_copy(step, side, apart):
         far_to = flip(far_index, apart)
         return remote(
-            summed.at[step, far_to],
-            arrived.at[apart - 1, flip(far_index, step)],
-            sum_send.at[step, apart - 1],
-            sum_recv.at[step, apart - 1],
+            summed.at[step * 2 + side, far_to],
+            arrived.at[apart - 1, columns_of(step, side)],
+            sum_send.at[step * 2 + side, apart - 1],
+            sum_recv.at[step * 2 + side, apart - 1],
             place(far_to, near_index, tp_index),
         )
 
-    def finish(step):
-        total = part[step, :, tp_index].astype(jnp.float32)
+    def finish(step, side):
+        total = part[step * 2 + side, :, tp_index].astype(jnp.float32)
         for other_tp in range(1, tp_count):
-            part_copy(step, other_tp).wait_recv()
-            total = total + other[step, other_tp - 1].astype(jnp.float32)
-        summed[step] = total.astype(summed.dtype)
+            with jax.named_scope(f"wait_part{step}_{side}"):
+                part_copy(step, side, other_tp).wait_recv()
+            total = total + other[step * 2 + side, other_tp - 1].astype(jnp.float32)
+        summed[step * 2 + side] = total.astype(summed.dtype)
         for apart in range(1, far):
-            sum_copy(step, apart).start()
-        own_sum[flip(far_index, step)] = summed[step, far_index]
-
-    for step in range(1, far):
-        take((2,), step, 0)
-        for role in relay_roles(step - 1):
-            take((2,), step - 1, role)
-    for role in relay_roles(far - 1):
-        take((2,), far - 1, role)
-    for step in range(far):
-        take_group((2,), step)
-        start = aligned(flip(far_index, step), chunk)
+            sum_copy(step, side, apart).start()
+        own_sum[columns_of(step, side)] = summed[step * 2 + side, far_index]
+
+    def down_part(step, side):
+        for role in range(side * near // 2, (side + 1) * near // 2):
+            take((2,), step, role)
+        start = aligned(columns_of(step, side), half)
         product = lax.dot_general(
             hidden[...],
-            down_all[pl.ds(start, chunk), :],
+            down_all[pl.ds(start, half), :],
             (((1,), (1,)), ((), ())),
             preferred_element_type=jnp.float32,
         )
-        part[step] = product.reshape(far, tp_count, own_rows, chunk).astype(part.dtype)
+        with jax.named_scope(f"downdot{step}_{side}"):
+            part[step * 2 + side] = product.reshape(far, tp_count, own_rows, half).astype(part.dtype)
         for other_tp in range(1, tp_count):
-            part_copy(step, other_tp).start()
-        if step:
-            finish(step - 1)
-    finish(far - 1)
-
-    for step in range(far):
+            part_copy(step, side, other_tp).start()
+
+    if far > 2:
+        take((2,), 2, 0)
+    relay((2,), 1)
+    order = [0, 1] + list(reversed(range(2, far)))
+    parts = [(step, side) for step in order for side in range(2)]
+    for number, (step, side) in enumerate(parts):
+        if side == 0:
+            for later in order[order.index(step) + 1 :][:1]:
+                take((2,), later, 0)
+                relay((2,), later)
+        down_part(step, side)
+        if number:
+            finish(*parts[number - 1])
+    finish(*parts[-1])
+
+    for step, side in parts:
         for apart in range(1, far):
-            remote(
-                summed.at[step, 0],
-                arrived.at[apart - 1, flip(flip(far_index, apart), step)],
-                sum_send.at[step, apart - 1],
-                sum_recv.at[step, apart - 1],
-                place(flip(far_index, apart), near_index, tp_index),
-            ).wait_recv()
-    for place_of in range(far):
-        span = pl.ds(place_of * chunk, chunk)
+            with jax.named_scope(f"wait_sum{step}_{side}_{apart}"):
+                remote(
+                    summed.at[step * 2 + side, 0],
+                    arrived.at[apart - 1, columns_of(step, side)],
+                    sum_send.at[step * 2 + side, apart - 1],
+                    sum_recv.at[step * 2 + side, apart - 1],
+                    place(flip(far_index, apart), near_index, tp_index),
+                ).wait_recv()
+    for place_of in range(2 * far):
+        span = pl.ds(place_of * half, half)
         channel = own_sum[place_of].astype(jnp.float32)
         for apart in range(1, far):
             channel = channel + arrived[apart - 1, place_of].astype(jnp.float32)
@@ -612,19 +685,23 @@
                 lambda number: far_copy(matrix, step, number).wait_send(),
             )
         for step in range(far):
-            for role, bit in near_sends(step):
+            for role, bit in near_sends(step + matrix):
                 by_count(
                     own_count,
                     lambda number: near_copy(matrix, step, role, bit, number).wait_send(),
                 )
+    for role, bit in rows_sends():
+        for piece in range(pieces):
+            rows_copy(role, bit, piece).wait_send()
     for step in range(far):
-        if step:
-            rows_copy(step).wait_send()
         for other_tp in range(1, tp_count):
-            pair_copy(step, other_tp).wait_send()
-            part_copy(step, other_tp).wait_send()
+            for piece in range(pieces):
+                pair_copy(step, other_tp, piece).wait_send()
+    for step, side in parts:
+        for other_tp in range(1, tp_count):
+            part_copy(step, side, other_tp).wait_send()
         for apart in range(1, far):
-            sum_copy(step, apart).wait_send()
+            sum_copy(step, side, apart).wait_send()
 
 
 def shards(
@@ -680,6 +757,7 @@
         in_specs=[vmem] * 11 + [anywhere] * 5,
         out_specs=vmem,
         scratch_shapes=[
+            pltpu.VMEM((tp_count, own_rows, key_width), bf16),
             pltpu.VMEM((tp_count, sp_count, own_rows, key_width), bf16),
             pltpu.VMEM((heads * row_count, key_width), bf16),
             pltpu.VMEM((row_count, key_total), f32),
@@ -697,11 +775,11 @@
             pltpu.VMEM((row_total, width), f32),
             pltpu.VMEM((row_total, width), f32),
             pltpu.VMEM((row_total, width), bf16),
-            pltpu.VMEM((far, far, tp_count, own_rows, chunk), bf16),
-            pltpu.VMEM((far, others, far, own_rows, chunk), bf16),
-            pltpu.VMEM((far, far, own_rows, chunk), bf16),
-            pltpu.VMEM((far - 1, far, own_rows, chunk), bf16),
-            pltpu.VMEM((far, own_rows, chunk), bf16),
+            pltpu.VMEM((2 * far, far, tp_count, own_rows, chunk // 2), bf16),
+            pltpu.VMEM((2 * far, others, far, own_rows, chunk // 2), bf16),
+            pltpu.VMEM((2 * far, far, own_rows, chunk // 2), bf16),
+            pltpu.VMEM((far - 1, 2 * far, own_rows, chunk // 2), bf16),
+            pltpu.VMEM((2 * far, own_rows, chunk // 2), bf16),
             dma((3,)),
             dma((2,)),
             dma((3, far)),
@@ -711,14 +789,14 @@
             dma((far, near)),
             dma((far + 1, others)),
             dma((far + 1, others)),
-            dma((far,)),
-            dma((far,)),
-            dma((far, others)),
-            dma((far, others)),
-            dma((far, others)),
-            dma((far, others)),
-            dma((far, far - 1)),
-            dma((far, far - 1)),
+            dma((far - 1, 2)),
+            dma((far, 2)),
+            dma((far, others, 2)),
+            dma((far, others, 2)),
+            dma((2 * far, others)),
+            dma((2 * far, others)),
+            dma((2 * far, far - 1)),
+            dma((2 * far, far - 1)),
         ],
         compiler_params=pltpu.CompilerParams(
             collective_id=0, has_side_effects=True, vmem_limit_bytes=58 * 1024 * 1024
@@ -728,13 +806,13 @@
         query_small,
         query_large,
         latent,
-        rope_key,
+        rope_key.T,
         jnp.asarray(rates[None, :], f32),
         key_up_small,
         value_up_small,
         key_up_large,
         value_up_large,
-        norm_gain[None, :],
+        norm_gain,
         out_small,
         out_large,
         gate_weight,

time: 125 us -> 106 us (0.85)
  Pallas kernels: 120 us -> 105 us
  local copies, waits for them, and re-layouts: 4.36 us -> 1.67 us
    pallas_call x1, Pallas kernels: 120 us -> 105 us  [shards(): pl.pallas_call(functools.partial(mixer, plan), out_shape=jax.ShapeDtypeSt...]
    unnamed x2 -> x1, local copies, waits for them, and re-layouts: 3.08 us -> 1.67 us
    broadcast_in_dim x1 -> x0, local copies, waits for them, and re-layouts: 1.28 us -> none  [shards(): norm_gain[None, :]]
where the time goes in v1:
time: 106 us
  Pallas kernels  105 us (99%)
  local copies, waits for them, and re-layouts  1.67 us (2%)
    pallas_call x1, Pallas kernels, shards(): pl.pallas_call(functools.partial(mixer, plan), out_shape=jax.ShapeDtypeSt...  105 us

profile of v1, /device:TPU:0, one launch (start us, length us, event | category | flops | bytes accessed | tf_op | source)
XLA Modules:
  0.0 106.2 jit_solution(6151261877390264129)
XLA Ops:
  0.0 104.5 %shard_map.154 = bf16[64,2048]{1,0:T(8,128)(2,1)} custom-call(bf16[64,2048]{1,0:T(8,128)(2,1)} %residual.1, bf16[128,384]{1,0:T(8,128)(2,1)} %query_small.1, bf16[128,640]{1,0:T(8,128)(2,1)} %query_large.1, bf16[128,256]{1,0:T(8,128)(2,1)} %latent.1, bf16[32,128]{1,0:T(8,128)(2,1)} %bitcast.1, f32[1,16]{1,0:T(1,128)} %constant.2.clone.turn_rates, ...), custom_call_target="tpu_custom_call" | custom-call | tf_op jit(solution)/shard_map/pallas_call | solution.py:754
  104.5 1.7 %copy.18 = bf16[64,2048]{1,0:T(8,128)(2,1)} copy(bf16[64,2048]{1,0:T(8,128)(2,1)} %shard_map.154) | data formatting | bytes 524288

commit v2 on v1

--- a/solution.py
+++ b/solution.py
@@ -36,6 +36,23 @@
 
 def mixer(
     plan,
+    residual_in,
+    query_small_in,
+    query_large_in,
+    latent_in,
+    rope_key_in,
+    turn_rates_in,
+    key_up_small_in,
+    value_up_small_in,
+    key_up_large_in,
+    value_up_large_in,
+    gain_in,
+    out_small,
+    out_large,
+    gate,
+    up,
+    down,
+    out,
     residual,
     query_small,
     query_large,
@@ -47,12 +64,6 @@
     key_up_large,
     value_up_large,
     gain,
-    out_small,
-    out_large,
-    gate,
-    up,
-    down,
-    out,
     keys_own,
     keys_all,
     queries,
@@ -78,6 +89,7 @@
     own_sum,
     copy_sem,
     out_sem,
+    small_sem,
     far_send,
     near_send,
     weight_recv,
@@ -156,8 +168,8 @@
         return remote(
             source(matrix, far_to, number),
             block(matrix, far_index, near_index, number),
-            far_send.at[matrix, step],
-            weight_recv.at[matrix, step, 0],
+            far_send.at[matrix],
+            weight_recv.at[slot(matrix, step, 0)],
             place(far_to, near_index, tp_index),
         )
 
@@ -173,6 +185,15 @@
                 sends.append((role, bit))
         return sends
 
+    slots = {}
+
+    def is_leaf(matrix, step, role):
+        return role > 0 and all(sender != role for sender, _ in near_sends(step + matrix))
+
+    def slot(matrix, step, role):
+        shared = matrix < 2 and is_leaf(matrix, step, role)
+        return slots.setdefault(("leaf", step) if shared else (matrix, step, role), len(slots))
+
     def near_copy(matrix, step, role, bit, number):
         far_from = flip(far_index, step)
         near_from = flip(near_index, role)
@@ -181,8 +202,8 @@
         return remote(
             source(matrix, far_index, number) if direct else target,
             target,
-            near_send.at[matrix, step, near_sends(step + matrix).index((role, bit))],
-            weight_recv.at[matrix, step, role | 1 << bit],
+            near_send.at[matrix],
+            weight_recv.at[slot(matrix, step, role | 1 << bit)],
             place(far_index, flip(near_index, 1 << bit), tp_index),
         )
 
@@ -215,7 +236,7 @@
                     target,
                     target,
                     copy_sem.at[matrix],
-                    weight_recv.at[matrix, step, role],
+                    weight_recv.at[slot(matrix, step, role)],
                     place(far_index, flip(near_index, 1), tp_index),
                 ).wait_recv()
 
@@ -240,8 +261,24 @@
                 take((matrix,), step, role)
 
     def take_group(matrices, step):
-        for role in range(near):
-            take(matrices, step, role)
+        leaves_of = [
+            (matrix, role)
+            for matrix in matrices
+            for role in range(near)
+            if is_leaf(matrix, step, role)
+        ]
+        for matrix in matrices:
+            for role in range(near):
+                if (matrix, role) not in leaves_of:
+                    take((matrix,), step, role)
+
+        def act(number):
+            rows = gate_all.at[pl.ds(0, len(leaves_of) * depth), pl.ds(0, number * LANES)]
+            pltpu.make_async_copy(rows, rows, weight_recv.at[slot(*shared)]).wait()
+
+        shared = (leaves_of[0][0], step, leaves_of[0][1])
+        with jax.named_scope(f"wait_leaves_s{step}"):
+            by_count(own_count, act)
 
     barrier = pltpu.get_barrier_semaphore()
     peers = [place(flip(far_index, step), near_index, tp_index) for step in range(1, far)]
@@ -249,6 +286,33 @@
     peers += [place(far_index, near_index, flip(tp_index, j)) for j in range(1, tp_count)]
     for peer in peers:
         pl.semaphore_signal(barrier, inc=1, device_id=peer, device_id_type=MESH)
+    loads = [
+        pltpu.make_async_copy(source_ref, held_ref, small_sem.at[place_of])
+        for place_of, (source_ref, held_ref) in enumerate(
+            (
+                (residual_in, residual),
+                (query_small_in, query_small),
+                (query_large_in, query_large),
+                (latent_in, latent),
+                (rope_key_in, rope_key),
+                (turn_rates_in, turn_rates),
+                (key_up_small_in, key_up_small),
+                (value_up_small_in, value_up_small),
+                (key_up_large_in, key_up_large),
+                (value_up_large_in, value_up_large),
+                (gain_in, gain),
+            )
+        )
+    ]
+    first_loads = (3, 4, 5)
+    for number in first_loads:
+        loads[number].start()
+    for number, load in enumerate(loads):
+        if number not in first_loads:
+            load.start()
+    for number in first_loads:
+        loads[number].wait()
+
     rates = turn_rates[...]
 
     def turning(first, count):
@@ -293,17 +357,22 @@
         return remote(
             key_block(0, 0),
             key_block(0, 0),
-            keys_send.at[step, near - 1],
+            keys_send.at[0],
             keys_recv.at[step, 0],
             place(flip(far_index, step), near_index, tp_index),
         )
+
+    def key_slot(step, role):
+        if role == 0:
+            return step, 0
+        return (step, 1 + relay_roles(step).index(role)) if role in relay_roles(step) else (0, 0)
 
     def key_near(step, role, bit):
         return remote(
             key_block(step, role),
             key_block(step, role),
-            keys_send.at[step, near_sends(step).index((role, bit))],
-            keys_recv.at[step, role | 1 << bit],
+            keys_send.at[0],
+            keys_recv.at[key_slot(step, role | 1 << bit)],
             place(far_index, flip(near_index, 1 << bit), tp_index),
         )
 
@@ -318,18 +387,17 @@
             key_block(step, role),
             key_block(step, role),
             copy_sem.at[0],
-            keys_recv.at[step, role],
+            keys_recv.at[key_slot(step, role)],
             place(far_index, flip(near_index, 1), tp_index),
         ).wait_recv()
         key_forward(step, role)
 
-    def key_pair(step, other_tp):
-        group = keys_all.at[tp_index, pl.ds(flip(far_index, step) * near, near)]
+    def key_pair(other_tp):
         return remote(
-            group,
-            group,
-            mixed_send.at[step, other_tp - 1],
-            mixed_recv.at[step, other_tp - 1],
+            keys_all.at[tp_index],
+            keys_all.at[tp_index],
+            mixed_send.at[0, other_tp - 1],
+            mixed_recv.at[0, other_tp - 1],
             place(far_index, near_index, flip(tp_index, other_tp)),
         )
 
@@ -359,6 +427,10 @@
         copy.start()
     for matrix in range(3):
         by_count(own_count, lambda number: own_copy(matrix, number).start())
+
+    for number, load in enumerate(loads):
+        if number not in first_loads:
+            load.wait()
 
     groups = []
     lifted = 0
@@ -396,30 +468,24 @@
     query_pos = first_row + lax.broadcasted_iota(jnp.int32, (row_count, 1), 0)
     bias[...] = jnp.where(key_pos <= query_pos, 0.0, big_negative)
 
-    def key_group(step):
-        for role in range(1, near):
-            if role not in relay_roles(step):
-                key_take(step, role)
-        for other_tp in range(1, tp_count):
-            key_pair(step, other_tp).start()
-
     for step in range(1, far):
         key_take(step, 0)
         for role in relay_roles(step - 1):
             key_take(step - 1, role)
-        if step > 1:
-            key_group(step - 2)
     relay(pairs, 0)
     for role in relay_roles(far - 1):
         key_take(far - 1, role)
     take(pairs, 1, 0)
     forward(2, 0, 0)
-    for step in range(max(far - 2, 0), far):
-        key_group(step)
-    for step in range(far):
-        for other_tp in range(1, tp_count):
-            with jax.named_scope('wait_keypair'):
-                key_pair(step, other_tp).wait_recv()
+    key_leaves = far * near - far - sum(len(relay_roles(step)) for step in range(far))
+    leaf_blocks = keys_all.at[0, pl.ds(0, key_leaves)]
+    with jax.named_scope("wait_keyleaves"):
+        pltpu.make_async_copy(leaf_blocks, leaf_blocks, keys_recv.at[0, 0]).wait()
+    for other_tp in range(1, tp_count):
+        key_pair(other_tp).start()
+    for other_tp in range(1, tp_count):
+        with jax.named_scope("wait_keypair"):
+            key_pair(other_tp).wait_recv()
 
     for index, (first_head, head, count, size, value_up, attended) in enumerate(groups):
         rows = pl.ds(first_head * row_count, count * row_count)
@@ -463,16 +529,14 @@
         return remote(
             mixed_other.at[0, other_tp - 1],
             mixed_other.at[1, other_tp - 1],
-            mixed_send.at[far, other_tp - 1],
-            mixed_recv.at[far, other_tp - 1],
+            mixed_send.at[1, other_tp - 1],
+            mixed_recv.at[1, other_tp - 1],
             place(far_index, near_index, tp_to),
         )
 
     for other_tp in range(1, tp_count):
         mixed_other[0, other_tp - 1] = mixed_part[flip(tp_index, other_tp)].astype(jnp.bfloat16)
         mixed_copy(other_tp).start()
-    for step in range(2, far):
-        take(pairs, step, 0)
     mixed = mixed_part[tp_index]
     for other_tp in range(1, tp_count):
         with jax.named_scope('wait_mixed'):
@@ -505,7 +569,7 @@
         return remote(
             rows_part(role, piece),
             rows_part(role, piece),
-            rows_send.at[rows_sends().index((role, bit)), piece],
+            rows_send.at[0],
             rows_recv.at[role | 1 << bit, piece],
             place(flip(far_index, 1 << bit), near_index, tp_index),
         )
@@ -514,8 +578,8 @@
         return remote(
             rows_part(role, piece),
             rows_part(role, piece),
-            pair_send.at[role, other_tp - 1, piece],
-            pair_recv.at[role, other_tp - 1, piece],
+            pair_send.at[other_tp - 1],
+            pair_recv.at[other_tp - 1],
             place(far_index, near_index, flip(tp_index, other_tp)),
         )
 
@@ -544,6 +608,8 @@
         start_far(2, step)
     relayed = sorted({role for role, _ in rows_sends() if role}, reverse=True)
     leaves = [role for role in range(1, far) if role not in relayed]
+    for step in range(2, far):
+        take(pairs, step, 0)
     relay((2,), 0)
     for step in range(2, far // 2 + 1):
         relay(pairs, step)
@@ -558,11 +624,11 @@
         rows_take(role)
     for step in reversed(range(3, far)):
         take((2,), step, 0)
-    for role in range(far):
-        for other_tp in range(1, tp_count):
-            for piece in range(pieces):
-                with jax.named_scope(f"wait_pair{role}"):
-                    pair_copy(role, other_tp, piece).wait_recv()
+    for other_tp in range(1, tp_count):
+        with jax.named_scope("wait_pair"):
+            pltpu.make_async_copy(
+                rows_all.at[:, 0], rows_all.at[:, 0], pair_recv.at[other_tp - 1]
+            ).wait()
 
     tile = 2 * LANES if width % (2 * LANES) == 0 else LANES
     for step in range(far):
@@ -590,12 +656,17 @@
         top = near // 2
         return flip(far_index, step) * 2 + lax.rem(lax.div(near_index, top) + side, 2)
 
+    def columns_of_far(step, side, apart):
+        top = near // 2
+        group = flip(flip(far_index, apart), step)
+        return group * 2 + lax.rem(lax.div(near_index, top) + side, 2)
+
     def part_copy(step, side, other_tp):
         tp_to = flip(tp_index, other_tp)
         return remote(
             part.at[step * 2 + side, :, tp_to],
             other.at[step * 2 + side, other_tp - 1],
-            part_send.at[step * 2 + side, other_tp - 1],
+            part_send.at[other_tp - 1],
             part_recv.at[step * 2 + side, other_tp - 1],
             place(far_index, near_index, tp_to),
         )
@@ -605,8 +676,8 @@
         return remote(
             summed.at[step * 2 + side, far_to],
             arrived.at[apart - 1, columns_of(step, side)],
-            sum_send.at[step * 2 + side, apart - 1],
-            sum_recv.at[step * 2 + side, apart - 1],
+            sum_send.at[0],
+            sum_recv.at[step * 2 + side],
             place(far_to, near_index, tp_index),
         )
 
@@ -619,7 +690,7 @@
         summed[step * 2 + side] = total.astype(summed.dtype)
         for apart in range(1, far):
             sum_copy(step, side, apart).start()
-        own_sum[columns_of(step, side)] = summed[step * 2 + side, far_index]
+        own_sum[columns_of(step, side)] = summed[step * 2 + side, far_index].astype(jnp.float32)
 
     def down_part(step, side):
         for role in range(side * near // 2, (side + 1) * near // 2):
@@ -638,70 +709,54 @@
 
     if far > 2:
         take((2,), 2, 0)
-    relay((2,), 1)
     order = [0, 1] + list(reversed(range(2, far)))
     parts = [(step, side) for step in order for side in range(2)]
     for number, (step, side) in enumerate(parts):
-        if side == 0:
-            for later in order[order.index(step) + 1 :][:1]:
-                take((2,), later, 0)
-                relay((2,), later)
         down_part(step, side)
+        if number + 1 < far:
+            relay((2,), order[number + 1])
         if number:
             finish(*parts[number - 1])
     finish(*parts[-1])
 
+    def await_bytes(ref, semaphore):
+        pltpu.make_async_copy(ref, ref, semaphore).wait()
+
+    await_bytes(keys_all.at[0, pl.ds(0, far * near - 1)], keys_send.at[0])
+    for other_tp in range(1, tp_count):
+        key_pair(other_tp).wait_send()
+        mixed_copy(other_tp).wait_send()
+        await_bytes(rows_all.at[:, 0], pair_send.at[other_tp - 1])
+        await_bytes(other.at[:, 0], part_send.at[other_tp - 1])
+    for matrix in range(3):
+
+        def await_far(number):
+            columns = pl.ds(0, (tiles - number) * LANES)
+            await_bytes(inputs[matrix].at[:, columns], far_send.at[matrix])
+
+        def await_near(number):
+            rows = pl.ds(0, far * (near - 1) * depth)
+            await_bytes(held[matrix].at[rows, pl.ds(0, number * LANES)], near_send.at[matrix])
+
+        if tiles % far == 0:
+            await_far(wide)
+        else:
+            for number in (wide - 1, wide):
+                pl.when(own_count == number)(functools.partial(await_far, number))
+        by_count(own_count, await_near)
+    await_bytes(rows_all.at[pl.ds(0, far - 1), 0], rows_send.at[0])
     for step, side in parts:
+        with jax.named_scope(f"wait_sum{step}_{side}"):
+            await_bytes(arrived.at[:, 0], sum_recv.at[step * 2 + side])
         for apart in range(1, far):
-            with jax.named_scope(f"wait_sum{step}_{side}_{apart}"):
-                remote(
-                    summed.at[step * 2 + side, 0],
-                    arrived.at[apart - 1, columns_of(step, side)],
-                    sum_send.at[step * 2 + side, apart - 1],
-                    sum_recv.at[step * 2 + side, apart - 1],
-                    place(flip(far_index, apart), near_index, tp_index),
-                ).wait_recv()
+            columns = columns_of_far(step, side, apart)
+            own_sum[columns] = own_sum[columns] + arrived[apart - 1, columns].astype(jnp.float32)
     for place_of in range(2 * far):
         span = pl.ds(place_of * half, half)
-        channel = own_sum[place_of].astype(jnp.float32)
-        for apart in range(1, far):
-            channel = channel + arrived[apart - 1, place_of].astype(jnp.float32)
-        channel = channel.astype(jnp.bfloat16).astype(jnp.float32)
+        channel = own_sum[place_of].astype(jnp.bfloat16).astype(jnp.float32)
         out[:, span] = (stream[:, span].astype(jnp.float32) + 0.5 * channel).astype(out.dtype)
 
-    for step in range(far):
-        if step:
-            key_far(step).wait_send()
-        for role, bit in near_sends(step):
-            key_near(step, role, bit).wait_send()
-        for other_tp in range(1, tp_count):
-            key_pair(step, other_tp).wait_send()
-    for other_tp in range(1, tp_count):
-        mixed_copy(other_tp).wait_send()
-    for matrix in range(3):
-        for step in range(1, far):
-            by_count(
-                tile_count(flip(far_index, step)),
-                lambda number: far_copy(matrix, step, number).wait_send(),
-            )
-        for step in range(far):
-            for role, bit in near_sends(step + matrix):
-                by_count(
-                    own_count,
-                    lambda number: near_copy(matrix, step, role, bit, number).wait_send(),
-                )
-    for role, bit in rows_sends():
-        for piece in range(pieces):
-            rows_copy(role, bit, piece).wait_send()
-    for step in range(far):
-        for other_tp in range(1, tp_count):
-            for piece in range(pieces):
-                pair_copy(step, other_tp, piece).wait_send()
-    for step, side in parts:
-        for other_tp in range(1, tp_count):
-            part_copy(step, side, other_tp).wait_send()
-        for apart in range(1, far):
-            sum_copy(step, side, apart).wait_send()
+    await_bytes(summed.at[:, pl.ds(0, far - 1)], sum_send.at[0])
 
 
 def shards(
@@ -745,18 +800,33 @@
     small, large = out_small.shape[0], out_large.shape[0]
     heads = small // HEAD_SMALL + large // HEAD_LARGE
     rates = 1.0 / rope_base ** (np.arange(0, ROPE, 2, dtype=np.float32) / ROPE)
+    small_operands = (
+        residual,
+        query_small,
+        query_large,
+        latent,
+        rope_key.T,
+        jnp.asarray(rates[None, :], jnp.float32),
+        key_up_small,
+        value_up_small,
+        key_up_large,
+        value_up_large,
+        norm_gain,
+    )
     plan = (far, near, tp_count, depth, tiles, wide, width)
     bf16, f32 = jnp.bfloat16, jnp.float32
     others = max(tp_count - 1, 1)
+    slot_count = far * near + 2 * far * (near // 2) + far
     dma = pltpu.SemaphoreType.DMA
     vmem = pl.BlockSpec(memory_space=pltpu.VMEM)
     anywhere = pl.BlockSpec(memory_space=pl.ANY)
     return pl.pallas_call(
         functools.partial(mixer, plan),
         out_shape=jax.ShapeDtypeStruct((own_rows, model), bf16),
-        in_specs=[vmem] * 11 + [anywhere] * 5,
+        in_specs=[anywhere] * 16,
         out_specs=vmem,
-        scratch_shapes=[
+        scratch_shapes=[pltpu.VMEM(value.shape, value.dtype) for value in small_operands]
+        + [
             pltpu.VMEM((tp_count, own_rows, key_width), bf16),
             pltpu.VMEM((tp_count, sp_count, own_rows, key_width), bf16),
             pltpu.VMEM((heads * row_count, key_width), bf16),
@@ -779,40 +849,31 @@
             pltpu.VMEM((2 * far, others, far, own_rows, chunk // 2), bf16),
             pltpu.VMEM((2 * far, far, own_rows, chunk // 2), bf16),
             pltpu.VMEM((far - 1, 2 * far, own_rows, chunk // 2), bf16),
-            pltpu.VMEM((2 * far, own_rows, chunk // 2), bf16),
+            pltpu.VMEM((2 * far, own_rows, chunk // 2), f32),
             dma((3,)),
             dma((2,)),
-            dma((3, far)),
-            dma((3, far, near - 1)),
-            dma((3, far, near)),
-            dma((far, near)),
-            dma((far, near)),
-            dma((far + 1, others)),
-            dma((far + 1, others)),
-            dma((far - 1, 2)),
+            dma((len(small_operands),)),
+            dma((3,)),
+            dma((3,)),
+            dma((slot_count,)),
+            dma((1,)),
+            dma((far, max(near // 2, 2))),
+            dma((2, others)),
+            dma((2, others)),
+            dma((1,)),
             dma((far, 2)),
-            dma((far, others, 2)),
-            dma((far, others, 2)),
+            dma((others,)),
+            dma((others,)),
+            dma((others,)),
             dma((2 * far, others)),
-            dma((2 * far, others)),
-            dma((2 * far, far - 1)),
-            dma((2 * far, far - 1)),
+            dma((1,)),
+            dma((2 * far,)),
         ],
         compiler_params=pltpu.CompilerParams(
             collective_id=0, has_side_effects=True, vmem_limit_bytes=58 * 1024 * 1024
         ),
     )(
-        residual,
-        query_small,
-        query_large,
-        latent,
-        rope_key.T,
-        jnp.asarray(rates[None, :], f32),
-        key_up_small,
-        value_up_small,
-        key_up_large,
-        value_up_large,
-        norm_gain,
+        *small_operands,
         out_small,
         out_large,
         gate_weight,

time: 106 us -> 103 us (0.972)
  Pallas kernels: 105 us -> 101 us
    pallas_call x1, Pallas kernels: 105 us -> 101 us  [shards(): pl.pallas_call(functools.partial(mixer, plan), out_shape=jax.ShapeDtypeSt...]
where the time goes in v2:
time: 103 us
  Pallas kernels  101 us (98%)
  local copies, waits for them, and re-layouts  1.67 us (2%)
    pallas_call x1, Pallas kernels, shards(): pl.pallas_call(functools.partial(mixer, plan), out_shape=jax.ShapeDtypeSt...  101 us

profile of v2, /device:TPU:0, one launch (start us, length us, event | category | flops | bytes accessed | tf_op | source)
XLA Modules:
  0.0 102.7 jit_solution(8155546476474319583)
XLA Ops:
  0.0 101.1 %shard_map.154 = bf16[64,2048]{1,0:T(8,128)(2,1)} custom-call(bf16[64,2048]{1,0:T(8,128)(2,1)} %residual_in.1, bf16[128,384]{1,0:T(8,128)(2,1)} %query_small_in.1, bf16[128,640]{1,0:T(8,128)(2,1)} %query_large_in.1, bf16[128,256]{1,0:T(8,128)(2,1)} %latent_in.1, bf16[32,128]{1,0:T(8,128)(2,1)} %bitcast.1, f32[1,16]{1,0:T(1,128)} %constant.2.clone.turn_rates_in, ...), custom_call_target="tpu_custom_call" | custom-call | tf_op jit(solution)/shard_map/pallas_call | solution.py:823
  101.1 1.7 %copy.18 = bf16[64,2048]{1,0:T(8,128)(2,1)} copy(bf16[64,2048]{1,0:T(8,128)(2,1)} %shard_map.154) | data formatting | bytes 524288

commit v3 on v2

--- a/solution.py
+++ b/solution.py
@@ -412,8 +412,8 @@
     inner = lax.rem(lax.div(far_index, max(far // 2, 1)) + lax.div(far_index, max(far // 4, 1)), 2)
 
     def start_rest(steps):
-        for step in steps:
-            for matrix in pairs:
+        for matrix in pairs:
+            for step in steps:
                 start_far(matrix, step)
 
     pl.when(inner == 0)(lambda: start_rest(range(2, far)))
@@ -537,6 +537,8 @@
     for other_tp in range(1, tp_count):
         mixed_other[0, other_tp - 1] = mixed_part[flip(tp_index, other_tp)].astype(jnp.bfloat16)
         mixed_copy(other_tp).start()
+    for step in range(2, far):
+        take(pairs[:1], step, 0)
     mixed = mixed_part[tp_index]
     for other_tp in range(1, tp_count):
         with jax.named_scope('wait_mixed'):
@@ -609,16 +611,16 @@
     relayed = sorted({role for role, _ in rows_sends() if role}, reverse=True)
     leaves = [role for role in range(1, far) if role not in relayed]
     for step in range(2, far):
-        take(pairs, step, 0)
+        take(pairs[1:], step, 0)
     relay((2,), 0)
-    for step in range(2, far // 2 + 1):
-        relay(pairs, step)
+    for step in range(2, far):
+        relay(pairs[:1], step)
     for role in relayed:
         rows_take(role)
     if far > 2:
         start_far(2, 2)
-    for step in range(far // 2 + 1, far):
-        relay(pairs, step)
+    for step in range(2, far):
+        relay(pairs[1:], step)
     take((2,), 1, 0)
     for role in leaves:
         rows_take(role)
@@ -710,13 +712,15 @@
     if far > 2:
         take((2,), 2, 0)
     order = [0, 1] + list(reversed(range(2, far)))
-    parts = [(step, side) for step in order for side in range(2)]
-    for number, (step, side) in enumerate(parts):
+    parts = [(0, 0), (0, 1)] + [(step, side) for side in range(2) for step in order[1:]]
+    down_part(0, 0)
+    down_part(0, 1)
+    finish(0, 0)
+    for number, (step, side) in enumerate(parts[2:], 2):
+        if side == 0:
+            relay((2,), step)
+        finish(*parts[number - 1])
         down_part(step, side)
-        if number + 1 < far:
-            relay((2,), order[number + 1])
-        if number:
-            finish(*parts[number - 1])
     finish(*parts[-1])
 
     def await_bytes(ref, semaphore):

time: 103 us -> 100 us (0.971)
  Pallas kernels: 101 us -> 98.3 us
    pallas_call x1, Pallas kernels: 101 us -> 98.3 us  [shards(): pl.pallas_call(functools.partial(mixer, plan), out_shape=jax.ShapeDtypeSt...]
where the time goes in v3:
time: 100 us
  Pallas kernels  98.3 us (98%)
  local copies, waits for them, and re-layouts  1.67 us (2%)
    pallas_call x1, Pallas kernels, shards(): pl.pallas_call(functools.partial(mixer, plan), out_shape=jax.ShapeDtypeSt...  98.3 us

profile of v3, /device:TPU:0, one launch (start us, length us, event | category | flops | bytes accessed | tf_op | source)
XLA Modules:
  0.0 100.0 jit_solution(1897538114101340569)
XLA Ops:
  0.0 98.3 %shard_map.154 = bf16[64,2048]{1,0:T(8,128)(2,1)} custom-call(bf16[64,2048]{1,0:T(8,128)(2,1)} %residual_in.1, bf16[128,384]{1,0:T(8,128)(2,1)} %query_small_in.1, bf16[128,640]{1,0:T(8,128)(2,1)} %query_large_in.1, bf16[128,256]{1,0:T(8,128)(2,1)} %latent_in.1, bf16[32,128]{1,0:T(8,128)(2,1)} %bitcast.1, f32[1,16]{1,0:T(1,128)} %constant.2.clone.turn_rates_in, ...), custom_call_target="tpu_custom_call" | custom-call | tf_op jit(solution)/shard_map/pallas_call | solution.py:827
  98.3 1.7 %copy.18 = bf16[64,2048]{1,0:T(8,128)(2,1)} copy(bf16[64,2048]{1,0:T(8,128)(2,1)} %shard_map.154) | data formatting | bytes 524288

commit v4 on v3

--- a/solution.py
+++ b/solution.py
@@ -66,6 +66,7 @@
     gain,
     keys_own,
     keys_all,
+    turned_all,
     queries,
     bias,
     attended_small,
@@ -333,9 +334,23 @@
     first_row = sp_index * row_count
     query_table = turning(first_row, row_count)
     key_turn = turned(rope_key[...].T, query_table).astype(jnp.bfloat16)
-    key_pad = jnp.zeros((row_count, keys_all.shape[3] - latent_width - ROPE), jnp.bfloat16)
-    own_keys = jnp.concatenate([latent[...], key_turn, key_pad], axis=1)
-    keys_own[...] = own_keys.reshape(tp_count, own_rows, keys_all.shape[3])
+    fold = latent_width // ROPE
+    packed = keys_all.shape[3] == latent_width
+    packed_rows = own_rows // fold
+    if packed:
+        wide_turn = key_turn.astype(jnp.float32)
+        for half_of in range(tp_count):
+            first = half_of * own_rows
+            keys_own[half_of, :own_rows, :] = latent[first : first + own_rows, :]
+            pieces_of = [
+                wide_turn[first + j * packed_rows : first + (j + 1) * packed_rows]
+                for j in range(fold)
+            ]
+            keys_own[half_of, own_rows:, :] = jnp.concatenate(pieces_of, axis=1).astype(jnp.bfloat16)
+    else:
+        key_pad = jnp.zeros((row_count, keys_all.shape[3] - latent_width - ROPE), jnp.bfloat16)
+        own_keys = jnp.concatenate([latent[...], key_turn, key_pad], axis=1)
+        keys_own[...] = own_keys.reshape(tp_count, own_rows, keys_all.shape[3])
     keys_all[tp_index, sp_index] = keys_own[tp_index]
 
     if tiles % far:
@@ -441,7 +456,7 @@
         span_width = size + ROPE
         heads = query.shape[1] // span_width
         scale = float(span_width) ** -0.5 * math.log2(math.e)
-        pad = jnp.zeros((row_count, keys_all.shape[3] - latent_width - ROPE), jnp.bfloat16)
+        pad = jnp.zeros((row_count, queries.shape[1] - latent_width - ROPE), jnp.bfloat16)
         for head in range(heads):
             vector = query[:, head * span_width : (head + 1) * span_width]
             content = lax.dot_general(
@@ -487,12 +502,29 @@
         with jax.named_scope("wait_keypair"):
             key_pair(other_tp).wait_recv()
 
+    if packed:
+        for j in range(fold):
+            turned_part = keys_all[:, :, own_rows:, j * ROPE : (j + 1) * ROPE].astype(jnp.float32)
+            turned_all[:, j * packed_rows : (j + 1) * packed_rows, :] = turned_part.reshape(
+                tp_count * far * near, packed_rows, ROPE
+            )
+
     for index, (first_head, head, count, size, value_up, attended) in enumerate(groups):
         rows = pl.ds(first_head * row_count, count * row_count)
-        keys = keys_all[...].reshape(key_total, keys_all.shape[3])
+        keys = keys_all[:, :, :own_rows, :].reshape(key_total, keys_all.shape[3])
         scores = lax.dot_general(
-            queries[rows, :], keys, (((1,), (1,)), ((), ())), preferred_element_type=jnp.float32
-        )
+            queries[rows, : keys.shape[1]],
+            keys,
+            (((1,), (1,)), ((), ())),
+            preferred_element_type=jnp.float32,
+        )
+        if packed:
+            scores = scores + lax.dot_general(
+                queries[rows, latent_width : latent_width + ROPE],
+                turned_all[...].reshape(key_total, ROPE).astype(jnp.bfloat16),
+                (((1,), (1,)), ((), ())),
+                preferred_element_type=jnp.float32,
+            )
         masked = scores.reshape(count, row_count, key_total) + bias[...][None]
         masked = masked.reshape(count * row_count, key_total)
         weights = jnp.exp2(masked - jnp.max(masked, axis=1, keepdims=True))
@@ -801,6 +833,10 @@
     row_total = far * tp_count * own_rows
     key_total = sp_count * row_count
     key_width = -(-(latent_width + ROPE) // LANES) * LANES
+    fold = latent_width // ROPE
+    packed = latent_width % LANES == 0 and own_rows % (8 * fold) == 0
+    block_rows = own_rows + own_rows // fold if packed else own_rows
+    block_width = latent_width if packed else key_width
     small, large = out_small.shape[0], out_large.shape[0]
     heads = small // HEAD_SMALL + large // HEAD_LARGE
     rates = 1.0 / rope_base ** (np.arange(0, ROPE, 2, dtype=np.float32) / ROPE)
@@ -831,8 +867,9 @@
         out_specs=vmem,
         scratch_shapes=[pltpu.VMEM(value.shape, value.dtype) for value in small_operands]
         + [
-            pltpu.VMEM((tp_count, own_rows, key_width), bf16),
-            pltpu.VMEM((tp_count, sp_count, own_rows, key_width), bf16),
+            pltpu.VMEM((tp_count, block_rows, block_width), bf16),
+            pltpu.VMEM((tp_count, sp_count, block_rows, block_width), bf16),
+            pltpu.VMEM((tp_count * sp_count if packed else 1, own_rows, ROPE), f32),
             pltpu.VMEM((heads * row_count, key_width), bf16),
             pltpu.VMEM((row_count, key_total), f32),
             pltpu.VMEM((row_count, small), bf16),

time: 100 us -> 99.2 us (level)
  Pallas kernels: 98.3 us -> 97.3 us
    pallas_call x1, Pallas kernels: 98.3 us -> 97.3 us  [shards(): pl.pallas_call(functools.partial(mixer, plan), out_shape=jax.ShapeDtypeSt...]
where the time goes in v4:
time: 99.2 us; the launch traced here: 99 us
  Pallas kernels  97.3 us (98%)
  local copies, waits for them, and re-layouts  1.67 us (2%)
    pallas_call x1, Pallas kernels, shards(): pl.pallas_call(functools.partial(mixer, plan), out_shape=jax.ShapeDtypeSt...  97.3 us

profile of v4, /device:TPU:0, one launch (start us, length us, event | category | flops | bytes accessed | tf_op | source)
XLA Modules:
  0.0 99.0 jit_solution(17239389703877870086)
XLA Ops:
  0.0 97.3 %shard_map.154 = bf16[64,2048]{1,0:T(8,128)(2,1)} custom-call(bf16[64,2048]{1,0:T(8,128)(2,1)} %residual_in.1, bf16[128,384]{1,0:T(8,128)(2,1)} %query_small_in.1, bf16[128,640]{1,0:T(8,128)(2,1)} %query_large_in.1, bf16[128,256]{1,0:T(8,128)(2,1)} %latent_in.1, bf16[32,128]{1,0:T(8,128)(2,1)} %bitcast.1, f32[1,16]{1,0:T(1,128)} %constant.2.clone.turn_rates_in, ...), custom_call_target="tpu_custom_call" | custom-call | tf_op jit(solution)/shard_map/pallas_call | solution.py:863
  97.3 1.7 %copy.18 = bf16[64,2048]{1,0:T(8,128)(2,1)} copy(bf16[64,2048]{1,0:T(8,128)(2,1)} %shard_map.154) | data formatting | bytes 524288
